TPU v7x, 32 devices: a whole 2x2x4 slice. The times are simulated.
32 devices in a mesh: grp: 2 (over y), ep: 8 (over z, core), tp: 2 (over x).
Axes of the slice: x: 2, y: 2, z: 4, core: 2. Of those that a mesh axis runs over, the one named last changes fastest.
Arguments:
- resid_in: bfloat16 [176, 2048], P(('grp', 'ep')), parts along dimension 0, may hold values from -6 to 6
- norm_attn: float32 [2048], replicated, may hold values from 0.1 to 1.9
- norm_moe: float32 [2048], replicated, may hold values from 0.1 to 1.9
- w_query: bfloat16 [2048, 1024], P('ep', 'tp'), may hold values from -0.125 to 0.125
- w_key: bfloat16 [2048, 256], P('ep', 'tp'), may hold values from -0.125 to 0.125
- w_value: bfloat16 [2048, 256], P('ep', 'tp'), may hold values from -0.125 to 0.125
- head_offset: float32 [16], P('tp'), may hold values from 1.5 to 9.5
- kv_cache: bfloat16 [176, 1024, 4, 128], P(('grp', 'ep'), None, 'tp'), parts along dimension 0, may hold values from -6 to 6
- lengths: int32 [176], P(('grp', 'ep')), parts along dimension 0, may hold values from 128 to 1024, as said below
- w_output: bfloat16 [1024, 2048], P('tp', 'ep'), may hold values from -0.375 to 0.375
- routes: int32 [176, 4], P(('grp', 'ep')), parts along dimension 0, may hold values from 0 to 7, all different within a row; in each aligned block of 11 rows (0 to 10, 11 to 21, ...) at most 7 rows name the same one
- route_weights: float32 [176, 4], P(('grp', 'ep')), parts along dimension 0, may hold values from 0.2 to 1
- gate_experts: bfloat16 [8, 2048, 512], P('ep', None, 'tp'), may hold values from -0.125 to 0.125
- up_experts: bfloat16 [8, 2048, 512], P('ep', None, 'tp'), may hold values from -0.125 to 0.125
- down_experts: bfloat16 [8, 512, 2048], P('ep', 'tp'), may hold values from -0.25 to 0.25
- gate_shared: bfloat16 [2048, 512], P('ep', 'tp'), may hold values from -0.125 to 0.125
- up_shared: bfloat16 [2048, 512], P('ep', 'tp'), may hold values from -0.125 to 0.125
- down_shared: bfloat16 [512, 2048], P('tp', 'ep'), may hold values from -0.25 to 0.25
Outputs:
- layer_out: bfloat16 [176, 2048], P(('grp', 'ep'), 'tp'), parts along dimension 0
- new_rows: bfloat16 [176, 4, 128], P(('grp', 'ep'), 'tp'), parts along dimension 0
There are 2 independent parts, one for each index of `grp`. A program takes and returns all parts, laid end to end along the dimension named above; an argument that names none is the same for every part. Nothing has to cross between parts.
Inputs may be any that keep to these rules, and one draw needn't show every extreme that they name: `routes`: among the rows of one device no expert is named more than 7 times, and in every draw some expert is named exactly 7 times by one device's rows; a row names 4 different experts. Sequence b's new token follows cache positions 0 to lengths[b] - 1; the other positions are not read.
All inputs are finite; a program needn't handle non-finite values.
Results may differ from a plain program's by a relative error of at most 0.015.
Values may be sent and summed in bfloat16 or wider, within the bound.
No kernel may reach another device: no remote copies, remote signals or barrier semaphores. Data moves between devices by JAX's collectives and lax.ppermute only.
A program may use at most 64 MiB of HBM per device.

v0:
```python
import jax
import jax.numpy as jnp
from jax import lax
from jax.sharding import PartitionSpec as P

HEAD = 64
TOPK = 4
EPS = 1e-06


def rms_scale(row_block, gain):
    rows_wide = row_block.astype(jnp.float32)
    inverse = lax.rsqrt(jnp.mean(rows_wide * rows_wide, axis=-1, keepdims=True) + EPS)
    return rows_wide * inverse * gain


def stick_read(query, kv_cache, lengths, offsets):
    seq_count = query.shape[0]
    kv_local = kv_cache.shape[2]
    head_local = offsets.shape[0]
    per_group = head_local // kv_local
    cache_len = kv_cache.shape[1]
    grouped = query.reshape(seq_count, kv_local, per_group, HEAD)
    key_rows = kv_cache[:, :, :, :HEAD]
    value_rows = kv_cache[:, :, :, HEAD:]
    scores = jnp.einsum("skgd,slkd->skgl", grouped, key_rows, preferred_element_type=jnp.float32)
    scores = scores * HEAD ** (-0.5) - offsets.reshape(1, kv_local, per_group, 1)
    positions = lax.broadcasted_iota(jnp.int32, (seq_count, cache_len), 1)
    alive_mask = (positions < lengths[:, None])[:, None, None, :]
    remain = jnp.where(alive_mask, jax.nn.log_sigmoid(-scores), 0.0)
    suffix = lax.cumsum(remain, axis=3, reverse=True) - remain
    stick = jnp.where(alive_mask, jnp.exp(jax.nn.log_sigmoid(scores) + suffix), 0.0).astype(
        jnp.bfloat16
    )
    mixed_out = jnp.einsum("skgl,slkd->skgd", stick, value_rows, preferred_element_type=jnp.float32)
    return mixed_out.reshape(seq_count, head_local * HEAD).astype(jnp.bfloat16)


def on_device(
    resid_in,
    norm_attn,
    norm_moe,
    w_query,
    w_key,
    w_value,
    head_offset,
    kv_cache,
    lengths,
    w_output,
    routes,
    route_weights,
    gate_experts,
    up_experts,
    down_experts,
    gate_shared,
    up_shared,
    down_shared,
):
    tok_count = resid_in.shape[0]
    n_ep = lax.axis_size("ep")
    normed = rms_scale(resid_in, norm_attn).astype(jnp.bfloat16)
    k_cols = w_key.shape[1]
    pieces = (
        lax.all_gather(w_query, "ep", axis=0, tiled=True),
        lax.all_gather(w_key, "ep", axis=0, tiled=True),
        lax.all_gather(w_value, "ep", axis=0, tiled=True),
    )
    sliced = normed
    query_f, key_f, value_f = tuple(
        (
            jnp.dot(sliced, weight_piece, preferred_element_type=jnp.float32)
            for weight_piece in pieces
        )
    )
    query = query_f.astype(jnp.bfloat16)
    kv_local = k_cols // HEAD
    key_new = key_f.astype(jnp.bfloat16).reshape(tok_count, kv_local, HEAD)
    value_new = value_f.astype(jnp.bfloat16).reshape(tok_count, kv_local, HEAD)
    new_rows = jnp.concatenate([key_new, value_new], axis=2)
    attended = stick_read(query, kv_cache, lengths, head_offset)
    attn_part = jnp.dot(
        attended,
        lax.all_gather(w_output, "ep", axis=1, tiled=True),
        preferred_element_type=jnp.float32,
    ).astype(jnp.bfloat16)
    attn_sum = lax.psum(attn_part, "tp").astype(jnp.float32)
    resid_mid = (resid_in.astype(jnp.float32) + attn_sum).astype(jnp.bfloat16)
    normed_moe = rms_scale(resid_mid, norm_moe).astype(jnp.bfloat16)
    pieces = (
        lax.all_gather(gate_shared, "ep", axis=0, tiled=True),
        lax.all_gather(up_shared, "ep", axis=0, tiled=True),
    )
    sliced = normed_moe
    gate_s = jnp.dot(sliced, pieces[0], preferred_element_type=jnp.float32)
    up_s = jnp.dot(sliced, pieces[1], preferred_element_type=jnp.float32)
    hidden_shared = (jax.nn.silu(gate_s) * up_s).astype(jnp.bfloat16)
    shared_part = jnp.dot(
        hidden_shared,
        lax.all_gather(down_shared, "ep", axis=1, tiled=True),
        preferred_element_type=jnp.float32,
    ).astype(jnp.bfloat16)
    shared_out = lax.psum_scatter(shared_part, "tp", scatter_dimension=1, tiled=True).astype(
        jnp.float32
    )
    local_experts = gate_experts.shape[0]
    experts_all = local_experts * n_ep
    capacity = min(tok_count, tok_count * TOPK // experts_all + 2)
    flat_routes = routes.reshape(-1)
    expert_ids = lax.broadcasted_iota(jnp.int32, (1, experts_all), 1)
    onehot = (flat_routes[:, None] == expert_ids).astype(jnp.int32)
    slots = jnp.sum((jnp.cumsum(onehot, axis=0) - onehot) * onehot, axis=1)
    expert_grid = lax.broadcasted_iota(jnp.int32, (experts_all, capacity, 1), 0)
    slot_grid = lax.broadcasted_iota(jnp.int32, (experts_all, capacity, 1), 1)
    match = (
        (flat_routes[None, None, :] == expert_grid) & (slots[None, None, :] == slot_grid)
    ).astype(jnp.bfloat16)
    source_rows = jnp.repeat(normed_moe, TOPK, axis=0)
    outgoing = jnp.einsum(
        "ecr,rd->ecd", match, source_rows, preferred_element_type=jnp.float32
    ).astype(jnp.bfloat16)
    arrived = lax.all_to_all(outgoing, "ep", split_axis=0, concat_axis=0, tiled=True)
    slot_count = arrived.shape[1]
    grouped_in = arrived.reshape(n_ep, local_experts, slot_count, arrived.shape[2])
    gate_h = jnp.einsum(
        "secd,edf->secf", grouped_in, gate_experts, preferred_element_type=jnp.float32
    )
    up_h = jnp.einsum("secd,edf->secf", grouped_in, up_experts, preferred_element_type=jnp.float32)
    hidden_e = (jax.nn.silu(gate_h) * up_h).astype(jnp.bfloat16)
    down_h = jnp.einsum(
        "secf,efd->secd", hidden_e, down_experts, preferred_element_type=jnp.float32
    ).astype(jnp.bfloat16)
    summed = (
        lax.psum_scatter(down_h, "tp", scatter_dimension=3, tiled=True)
        .astype(jnp.float32)
        .astype(jnp.bfloat16)
    )
    summed = summed.reshape(n_ep * local_experts, slot_count, summed.shape[3])
    returned = lax.all_to_all(summed, "ep", split_axis=0, concat_axis=0, tiled=True)
    gathered_back = jnp.einsum("ecr,ecd->rd", match, returned, preferred_element_type=jnp.float32)
    col_width = gathered_back.shape[1]
    weighted = gathered_back.reshape(tok_count, TOPK, col_width) * route_weights[:, :, None]
    routed = jnp.sum(weighted, axis=1)
    own_cols = lax.dynamic_slice_in_dim(resid_mid, lax.axis_index("tp") * col_width, col_width, 1)
    layer_out = (own_cols.astype(jnp.float32) + shared_out + routed).astype(jnp.bfloat16)
    return (layer_out, new_rows)


def solution(mesh):
    return jax.shard_map(
        on_device,
        mesh=mesh,
        in_specs=(
            P(("grp", "ep"), None),
            P(),
            P(),
            P("ep", "tp"),
            P("ep", "tp"),
            P("ep", "tp"),
            P("tp"),
            P(("grp", "ep"), None, "tp", None),
            P(("grp", "ep")),
            P("tp", "ep"),
            P(("grp", "ep"), None),
            P(("grp", "ep"), None),
            P("ep", None, "tp"),
            P("ep", None, "tp"),
            P("ep", "tp", None),
            P("ep", "tp"),
            P("ep", "tp"),
            P("tp", "ep"),
        ),
        out_specs=(P(("grp", "ep"), "tp"), P(("grp", "ep"), "tp", None)),
        check_vma=False,
    )
```

profile of v0, /device:TPU:0, one launch (start us, length us, event | category | flops | bytes accessed | tf_op | source)
XLA Modules:
  0.0 270.2 jit_solution(16846753004733863255)
XLA Ops:
  7.2 0.7 all-gather.6.cloned.1.call-update
  8.0 0.7 all-gather.8.cloned.1.call-update
  8.7 0.7 all-gather.10.cloned.1.call-update
  9.4 1.0 fusion.33
  10.5 12.9 %fusion.66 = (bf16[11,1024,2,64]{3,2,1,0:T(2,128)(2,1)}, bf16[11,1024,2,64]{3,2,1,0:T(2,128)(2,1)}) fusion(bf16[11,1024,2,128]{3,2,1,0:T(2,128)(2,1)} %param.25), kind=kLoop, calls=%fused_computation.81 | loop fusion | bytes 11534336 | tf_op jit(solution)/shard_map/slice | solution.py:24
  24.1 17.4 %all-gather.6.cloned.1.call-done = bf16[2048,512]{1,0:T(8,128)(2,1)} async-done(((bf16[256,512]{1,0:T(8,128)(2,1)}), bf16[2048,512]{1,0:T(8,128)(2,1)}) %all-gather.6.cloned.1.call-update) | async-done | bytes 2097168 | tf_op jit(solution)/shard_map/all_gather | solution.py:64
  41.5 2.0 convolution_convert_fusion.4
  43.6 4.3 %fusion.26 = (f32[11,2,4,1024]{3,2,1,0:T(4,128)S(1)}, f32[11,2,4,1024]{3,2,1,0:T(4,128)S(1)}) fusion(pred[11,1024]{1,0:T(8,128)(4,1)S(1)} %iota_compare_fusion, f32[2,4]{1,0:T(2,128)S(1)} %sub.16, bf16[11,2,4,64]{3,2,1,0:T(4,128)(2,1)S(1)} %reshape.94, bf16[11,1024,2,64]{3,2,1,0:T(2,128)(2,1)} %get-tuple-element.4), kind=kOutput, calls=%fused_computation.31 | convolution fusion | flops 12435456 | bytes 3627040 | tf_op jit(solution)/shard_map/skgd,slkd->skgl/dot_general | solution.py:26
  48.0 108.9 %reduce-window.6 = f32[11,2,4,8,128]{4,3,2,1,0:T(8,128)S(1)} reduce-window(f32[11,2,4,8,128]{4,3,2,1,0:T(8,128)S(1)} %reshape.95, f32[]{:T(128)} %constant.15.clone.1), window={size=1x1x1x1x128 pad=0_0x0_0x0_0x0_0x0_127}, to_apply=%region_1.2 | reduce-window | flops 11444224 | bytes 720900 | tf_op jit(solution)/shard_map/reduce-window
  157.0 0.5 copy.31
  158.0 4.4 %fusion.11 = bf16[11,2,4,64]{3,2,1,0:T(4,128)(2,1)S(1)} fusion(bf16[11,1024,2,64]{3,2,1,0:T(2,128)(2,1)} %get-tuple-element.5, f32[11,2,4,1024]{3,2,1,0:T(4,128)S(1)} %reduce_window_sum.26, f32[11,2,4,1024]{3,2,1,0:T(4,128)S(1)} %get-tuple-element.7, pred[11,1024]{1,0:T(8,128)(4,1)S(1)} %iota_compare_fusion), kind=kOutput, calls=%fused_computation.12 | convolution fusion | flops 13342208 | bytes 3627008 | tf_op jit(solution)/shard_map/skgl,slkd->skgd/dot_general | solution.py:35
  162.5 2.0 convolution_convert_fusion.3
  164.5 8.8 %psum.7 = bf16[11,2048]{1,0:T(8,128)(2,1)S(1)} all-reduce(bf16[11,2048]{1,0:T(8,128)(2,1)S(1)} %convolution_convert_fusion.3), channel_id=1, replica_groups=mesh['grp'=2,'ep'=8,'tp'=2] {'tp'}, use_global_device_ids=true, to_apply=%region_3.4 | all-reduce | flops 22528 | bytes 90112 | tf_op jit(solution)/shard_map/psum | solution.py:86
  174.0 12.6 %all_to_all.10 = bf16[8,7,2048]{2,1,0:T(8,128)(2,1)S(1)} all-to-all(bf16[8,7,2048]{2,1,0:T(8,128)(2,1)S(1)} %copy.35), channel_id=1, replica_groups=mesh['grp'=2,'ep'=8,'tp'=2] {'ep'}, dimensions={0} | all-to-all | bytes 458752 | tf_op jit(solution)/shard_map/all_to_all | solution.py:121
  186.6 0.3 fusion.16
  187.0 1.6 fusion.18
  188.5 1.0 fusion.4
  189.6 0.5 all-gather.12.cloned.1.call-update
  190.2 0.5 all-gather.14.cloned.1.call-update
  190.8 14.9 %all_gather.26 = bf16[2048,128]{1,0:T(8,128)(2,1)S(1)} all-gather(bf16[256,128]{1,0:T(8,128)(2,1)S(1)} %copy-done.4), channel_id=1, replica_groups=mesh['grp'=2,'ep'=8,'tp'=2] {'ep'}, dimensions={0}, use_global_device_ids=true | all-gather | bytes 589824 | tf_op jit(solution)/shard_map/all_gather | solution.py:65
  205.8 0.2 convolution_convert_fusion.6
  206.1 16.9 %all_gather.27 = bf16[2048,128]{1,0:T(8,128)(2,1)S(1)} all-gather(bf16[256,128]{1,0:T(8,128)(2,1)S(1)} %copy-done.5), channel_id=1, replica_groups=mesh['grp'=2,'ep'=8,'tp'=2] {'ep'}, dimensions={0}, use_global_device_ids=true | all-gather | bytes 589824 | tf_op jit(solution)/shard_map/all_gather | solution.py:66
  223.0 0.2 convolution_convert_fusion.5
  223.3 0.7 pad_maximum_fusion
  224.0 1.5 fusion.67
  225.5 1.6 copy.38
  227.1 3.4 %all-to-all-start.1 = ((bf16[8,7,1024]{2,1,0:T(8,128)(2,1)}), bf16[8,7,1024]{2,1,0:T(8,128)(2,1)S(1)}, u32[]{:S(2)}, u32[]{:S(2)}) async-start(bf16[8,7,1024]{2,1,0:T(8,128)(2,1)} %copy.38), calls=%async_computation.3 | async-start | bytes 262144 | tf_op jit(solution)/shard_map/all_to_all | solution.py:138
  230.5 19.6 %all-gather.14.cloned.1.call-done = bf16[256,2048]{1,0:T(8,128)(2,1)} async-done(((bf16[256,256]{1,0:T(8,128)(2,1)}), bf16[256,2048]{1,0:T(8,128)(2,1)}) %all-gather.14.cloned.1.call-update) | async-done | bytes 1048592 | tf_op jit(solution)/shard_map/all_gather | solution.py:99
  250.1 2.9 %convolution_convert_fusion.2 = bf16[11,2048]{1,0:T(8,128)(2,1)} fusion(bf16[256,2048]{1,0:T(8,128)(2,1)} %all-gather.14.cloned.1.call-done, bf16[11,2048]{1,0:T(8,128)(2,1)S(1)} %fusion.32, bf16[2048,256]{1,0:T(8,128)(2,1)} %all-gather.12.cloned.1.call-done, f32[11,256]{1,0:T(8,128)S(1)} %fusion.67), kind=kOutput, calls=%fused_computation.7 | convolution fusion | flops 23108096 | bytes 2198528 | tf_op jit(solution)/shard_map/dot_general | solution.py:97
  253.1 0.2 convolution_bitcast_fusion
  253.5 8.5 %reduce-scatter.3.cloned.1.call-done = bf16[11,1024]{1,0:T(8,128)(2,1)} async-done(((bf16[11,2048]{1,0:T(8,128)(2,1)}), bf16[11,1024]{1,0:T(8,128)(2,1)}) %reduce-scatter.3.cloned.1.call-update) | async-done | bytes 22544 | tf_op jit(solution)/shard_map/reduce_scatter | solution.py:102
  262.0 1.4 add_convert_fusion
  (64 shorter events, 3.1 us)
Async XLA Ops:
  7.2 181.4 %copy-start = (bf16[1,256,2048]{2,1,0:T(8,128)(2,1)S(1)}, bf16[1,256,2048]{2,1,0:T(8,128)(2,1)}, u32[]{:S(2)}) copy-start(bf16[1,256,2048]{2,1,0:T(8,128)(2,1)} %param.32) | copy-start | bytes 3145732
  7.2 34.3 %all-gather.6.cloned.1.call-start = ((), (), s32[]{:S(2)}) async-start(), calls=%async_computation.4 | async-start | bytes 2359296 | tf_op jit(solution)/shard_map/all_gather | solution.py:64
  7.9 154.6 %all-gather.8.cloned.1.call-start = ((), (), s32[]{:S(2)}) async-start(), calls=%async_computation.5 | async-start | bytes 2359296 | tf_op jit(solution)/shard_map/all_gather | solution.py:83
  8.7 215.3 %all-gather.10.cloned.1.call-start = ((), (), s32[]{:S(2)}) async-start(), calls=%async_computation.6 | async-start | bytes 1179648 | tf_op jit(solution)/shard_map/all_gather | solution.py:90
  9.4 216.1 %reduce-scatter.5.cloned.1.call-start = ((), (), s32[]{:S(2)}) async-start(), calls=%async_computation.10 | async-start | bytes 344064 | tf_op jit(solution)/shard_map/reduce_scatter | solution.py:133
  10.4 13.0 %copy-start.9 = (s32[11]{0:T(128)S(1)}, s32[11]{0:T(128)}, u32[]{:S(2)}) copy-start(s32[11]{0:T(128)} %param.26) | copy-start | bytes 136
  10.4 13.1 %copy-start.10 = (f32[8]{0:T(128)S(1)}, f32[8]{0:T(128)}, u32[]{:S(2)}) copy-start(f32[8]{0:T(128)} %param.24) | copy-start | bytes 100
  10.4 13.2 %copy-start.7 = (s32[11,4]{0,1:T(4,128)S(1)}, s32[11,4]{0,1:T(4,128)}, u32[]{:S(2)}) copy-start(s32[11,4]{0,1:T(4,128)} %param.28) | copy-start | bytes 532
  10.5 31.0 %copy-start.1 = (bf16[11,2048]{1,0:T(8,128)(2,1)S(1)}, bf16[11,2048]{1,0:T(8,128)(2,1)}, u32[]{:S(2)}) copy-start(bf16[11,2048]{1,0:T(8,128)(2,1)} %param.18) | copy-start | bytes 135172
  10.5 31.0 %copy-start.3 = (f32[2048]{0:T(1024)S(1)}, f32[2048]{0:T(1024)}, u32[]{:S(2)}) copy-start(f32[2048]{0:T(1024)} %param.19) | copy-start | bytes 24580
  158.0 15.5 %copy-start.6 = (f32[2048]{0:T(1024)S(1)}, f32[2048]{0:T(1024)}, u32[]{:S(2)}) copy-start(f32[2048]{0:T(1024)} %param.20) | copy-start | bytes 24580
  158.0 28.6 %copy-start.2 = (bf16[1,2048,256]{2,1,0:T(8,128)(2,1)S(1)}, bf16[1,2048,256]{2,1,0:T(8,128)(2,1)}, u32[]{:S(2)}) copy-start(bf16[1,2048,256]{2,1,0:T(8,128)(2,1)} %param.31) | copy-start | bytes 3145732
  162.4 28.4 %copy-start.8 = (f32[11,4]{0,1:T(4,128)S(1)}, f32[11,4]{0,1:T(4,128)}, u32[]{:S(2)}) copy-start(f32[11,4]{0,1:T(4,128)} %param.29) | copy-start | bytes 532
  162.4 28.5 %copy-start.4 = (bf16[256,128]{1,0:T(8,128)(2,1)S(1)}, bf16[256,128]{1,0:T(8,128)(2,1)}, u32[]{:S(2)}) copy-start(bf16[256,128]{1,0:T(8,128)(2,1)} %param.22) | copy-start | bytes 196612
  162.4 43.7 %copy-start.5 = (bf16[256,128]{1,0:T(8,128)(2,1)S(1)}, bf16[256,128]{1,0:T(8,128)(2,1)}, u32[]{:S(2)}) copy-start(bf16[256,128]{1,0:T(8,128)(2,1)} %param.23) | copy-start | bytes 196612
  189.6 41.0 %all-gather.12.cloned.1.call-start = ((), (), s32[]{:S(2)}) async-start(), calls=%async_computation.7 | async-start | bytes 1179648 | tf_op jit(solution)/shard_map/all_gather | solution.py:91
  190.2 60.0 %all-gather.14.cloned.1.call-start = ((), (), s32[]{:S(2)}) async-start(), calls=%async_computation.8 | async-start | bytes 1179648 | tf_op jit(solution)/shard_map/all_gather | solution.py:99
  227.1 26.0 %all-to-all-start.1 = ((bf16[8,7,1024]{2,1,0:T(8,128)(2,1)}), bf16[8,7,1024]{2,1,0:T(8,128)(2,1)S(1)}, u32[]{:S(2)}, u32[]{:S(2)}) async-start(bf16[8,7,1024]{2,1,0:T(8,128)(2,1)} %copy.38), calls=%async_computation.3 | async-start | bytes 262144 | tf_op jit(solution)/shard_map/all_to_all | solution.py:138
  230.5 31.5 %reduce-scatter.3.cloned.1.call-start = ((), (), s32[]{:S(2)}) async-start(), calls=%async_computation.9 | async-start | bytes 98304 | tf_op jit(solution)/shard_map/reduce_scatter | solution.py:102
Sparse Core Ops, SparseCore 0:
  9.6 31.8 all-gather.5
  43.1 30.0 all-gather.7
  74.8 21.2 all-gather.9
  189.7 9.3 reduce-scatter.4
  200.5 24.5 all-gather.11
  226.6 23.5 all-gather.13
  253.2 8.7 reduce-scatter.2
where the time goes:
time: 271 us; the launch traced here: 270 us
  other arithmetic  113 us (42%)
  blocking collectives  53.2 us (20%)
  waiting for transfers between devices  48.6 us (18%)
  matrix products  20.8 us (8%)
  local copies, waits for them, and re-layouts  16.5 us (6%)
  between operations  14.4 us (5%)
  starting transfers between devices  3.64 us (1%)
    another operation x2, other arithmetic  109 us
    all_gather x1, waiting for transfers between devices, on_device(): lax.all_gather(down_shared, 'ep', axis=1, tiled=True)  19.6 us
    all_gather x1, waiting for transfers between devices, on_device(): lax.all_gather(w_query, 'ep', axis=0, tiled=True)  17.4 us
    all_gather x1, blocking collectives, on_device(): lax.all_gather(w_value, 'ep', axis=0, tiled=True)  16.9 us
    all_gather x1, blocking collectives, on_device(): lax.all_gather(w_key, 'ep', axis=0, tiled=True)  14.9 us
    slice x1, local copies, waits for them, and re-layouts, stick_read(): key_rows = kv_cache[:, :, :, :HEAD]  12.9 us
    all_to_all x1, blocking collectives, on_device(): lax.all_to_all(outgoing, 'ep', split_axis=0, concat_axis=0, tiled=True)  12.6 us
    psum x1, blocking collectives, on_device(): attn_sum = lax.psum(attn_part, 'tp').astype(jnp.float32)  8.79 us
  transfers between devices with their start and end apart: 8, of which 3 were waited for; matrix products, arithmetic and copies ran while one was open for 55% of the time, Pallas kernels for 0%

commit v1 on v0

--- a/solution.py
+++ b/solution.py
@@ -96,7 +96,7 @@
     hidden_shared = (jax.nn.silu(gate_s) * up_s).astype(jnp.bfloat16)
     shared_part = jnp.dot(
         hidden_shared,
-        lax.all_gather(down_shared, "ep", axis=1, tiled=True),
+        jnp.concatenate(lax.all_gather(down_shared, "ep"), axis=1),
         preferred_element_type=jnp.float32,
     ).astype(jnp.bfloat16)
     shared_out = lax.psum_scatter(shared_part, "tp", scatter_dimension=1, tiled=True).astype(

time: 271 us -> 254 us (0.937)
  waiting for transfers between devices: 48.6 us -> 30.2 us
    all_gather x1, waiting for transfers between devices: 19.6 us -> 0.01 us  [on_device(): lax.all_gather(down_shared, 'ep')]
    all_to_all x1, waiting for transfers between devices: 0.01 us -> 3.9 us  [on_device(): lax.all_to_all(summed, 'ep', split_axis=0, concat_axis=0, tiled=True)]
  transfers between devices with their start and end apart: 8 -> 8, of which waited for: 3 -> 3; matrix products, arithmetic and copies ran while one was open for 55% -> 60% of each run, Pallas kernels for 0% -> 0%
where the time goes in v1:
time: 254 us
  other arithmetic  113 us (44%)
  blocking collectives  52.9 us (21%)
  waiting for transfers between devices  30.2 us (12%)
  matrix products  21.4 us (8%)
  local copies, waits for them, and re-layouts  18 us (7%)
  between operations  14.4 us (6%)
  starting transfers between devices  3.64 us (1%)
    another operation x2, other arithmetic  109 us
    all_gather x1, waiting for transfers between devices, on_device(): lax.all_gather(w_query, 'ep', axis=0, tiled=True)  16.8 us
    all_gather x1, blocking collectives, on_device(): lax.all_gather(w_value, 'ep', axis=0, tiled=True)  16.6 us
    all_gather x1, blocking collectives, on_device(): lax.all_gather(w_key, 'ep', axis=0, tiled=True)  14.9 us
    slice x1, local copies, waits for them, and re-layouts, stick_read(): key_rows = kv_cache[:, :, :, :HEAD]  12.9 us
    all_to_all x1, blocking collectives, on_device(): lax.all_to_all(outgoing, 'ep', split_axis=0, concat_axis=0, tiled=True)  12.6 us
    psum x1, blocking collectives, on_device(): attn_sum = lax.psum(attn_part, 'tp').astype(jnp.float32)  8.79 us
    reduce_scatter x1, waiting for transfers between devices, on_device(): lax.psum_scatter(shared_part, 'tp', scatter_dimension=1, tiled=True)  6.32 us
  transfers between devices with their start and end apart: 8, of which 3 were waited for; matrix products, arithmetic and copies ran while one was open for 60% of the time, Pallas kernels for 0%

profile of v1, /device:TPU:0, one launch (start us, length us, event | category | flops | bytes accessed | tf_op | source)
XLA Modules:
  0.0 253.6 jit_solution(12424076745943716333)
XLA Ops:
  7.2 0.7 all-gather.7.cloned.1.call-update
  8.0 0.7 all-gather.9.cloned.1.call-update
  8.7 0.7 all-gather.15.cloned.1.call-update
  9.4 0.5 all-gather.11.cloned.1.call-update
  10.0 1.0 fusion.33
  11.1 12.9 %fusion.66 = (bf16[11,1024,2,64]{3,2,1,0:T(2,128)(2,1)}, bf16[11,1024,2,64]{3,2,1,0:T(2,128)(2,1)}) fusion(bf16[11,1024,2,128]{3,2,1,0:T(2,128)(2,1)} %param.25), kind=kLoop, calls=%fused_computation.81 | loop fusion | bytes 11534336 | tf_op jit(solution)/shard_map/slice | solution.py:24
  24.7 16.8 %all-gather.7.cloned.1.call-done = bf16[2048,512]{1,0:T(8,128)(2,1)} async-done(((bf16[256,512]{1,0:T(8,128)(2,1)}), bf16[2048,512]{1,0:T(8,128)(2,1)}) %all-gather.7.cloned.1.call-update) | async-done | bytes 2097168 | tf_op jit(solution)/shard_map/all_gather | solution.py:64
  41.5 2.0 convolution_convert_fusion.4
  43.6 5.0 %fusion.26 = (f32[11,2,4,1024]{3,2,1,0:T(4,128)S(1)}, f32[11,2,4,1024]{3,2,1,0:T(4,128)}) fusion(pred[11,1024]{1,0:T(8,128)(4,1)S(1)} %iota_compare_fusion, f32[2,4]{1,0:T(2,128)S(1)} %sub.16, bf16[11,2,4,64]{3,2,1,0:T(4,128)(2,1)S(1)} %reshape.100, bf16[11,1024,2,64]{3,2,1,0:T(2,128)(2,1)} %get-tuple-element.4), kind=kOutput, calls=%fused_computation.31 | convolution fusion | flops 12435456 | bytes 3627040 | tf_op jit(solution)/shard_map/skgd,slkd->skgl/dot_general | solution.py:26
  48.7 108.9 %reduce-window.6 = f32[11,2,4,8,128]{4,3,2,1,0:T(8,128)S(1)} reduce-window(f32[11,2,4,8,128]{4,3,2,1,0:T(8,128)S(1)} %reshape.101, f32[]{:T(128)} %constant.15.clone.1), window={size=1x1x1x1x128 pad=0_0x0_0x0_0x0_0x0_127}, to_apply=%region_1.2 | reduce-window | flops 11444224 | bytes 720900 | tf_op jit(solution)/shard_map/reduce-window
  157.7 0.5 copy.38
  158.7 4.5 %fusion.11 = bf16[11,2,4,64]{3,2,1,0:T(4,128)(2,1)S(1)} fusion(bf16[11,1024,2,64]{3,2,1,0:T(2,128)(2,1)} %get-tuple-element.5, f32[11,2,4,1024]{3,2,1,0:T(4,128)S(1)} %reduce_window_sum.26, f32[11,2,4,1024]{3,2,1,0:T(4,128)} %get-tuple-element.7, pred[11,1024]{1,0:T(8,128)(4,1)S(1)} %iota_compare_fusion), kind=kOutput, calls=%fused_computation.12 | convolution fusion | flops 13342208 | bytes 3627008 | tf_op jit(solution)/shard_map/skgl,slkd->skgd/dot_general | solution.py:35
  163.3 2.0 convolution_convert_fusion.3
  165.3 8.8 %psum.7 = bf16[11,2048]{1,0:T(8,128)(2,1)S(1)} all-reduce(bf16[11,2048]{1,0:T(8,128)(2,1)S(1)} %convolution_convert_fusion.3), channel_id=1, replica_groups=mesh['grp'=2,'ep'=8,'tp'=2] {'tp'}, use_global_device_ids=true, to_apply=%region_3.4 | all-reduce | flops 22528 | bytes 90112 | tf_op jit(solution)/shard_map/psum | solution.py:86
  174.8 12.6 %all_to_all.10 = bf16[8,7,2048]{2,1,0:T(8,128)(2,1)S(1)} all-to-all(bf16[8,7,2048]{2,1,0:T(8,128)(2,1)S(1)} %copy.43), channel_id=1, replica_groups=mesh['grp'=2,'ep'=8,'tp'=2] {'ep'}, dimensions={0} | all-to-all | bytes 458752 | tf_op jit(solution)/shard_map/all_to_all | solution.py:121
  187.4 0.3 fusion.16
  187.8 1.6 fusion.18
  189.3 1.0 fusion.4
  190.4 0.5 all-gather.13.cloned.1.call-update
  191.1 14.9 %all_gather.30 = bf16[2048,128]{1,0:T(8,128)(2,1)S(1)} all-gather(bf16[256,128]{1,0:T(8,128)(2,1)S(1)} %copy-done.4), channel_id=1, replica_groups=mesh['grp'=2,'ep'=8,'tp'=2] {'ep'}, dimensions={0}, use_global_device_ids=true | all-gather | bytes 589824 | tf_op jit(solution)/shard_map/all_gather | solution.py:65
  206.0 0.2 convolution_convert_fusion.6
  206.3 16.6 %all_gather.31 = bf16[2048,128]{1,0:T(8,128)(2,1)S(1)} all-gather(bf16[256,128]{1,0:T(8,128)(2,1)S(1)} %copy-done.5), channel_id=1, replica_groups=mesh['grp'=2,'ep'=8,'tp'=2] {'ep'}, dimensions={0}, use_global_device_ids=true | all-gather | bytes 589824 | tf_op jit(solution)/shard_map/all_gather | solution.py:66
  222.9 0.2 convolution_convert_fusion.5
  223.2 0.7 pad_maximum_fusion
  223.9 1.5 copy.41
  225.4 1.5 fusion.67
  226.9 1.6 copy.46
  228.5 3.4 %all-to-all-start.1 = ((bf16[8,7,1024]{2,1,0:T(8,128)(2,1)}), bf16[8,7,1024]{2,1,0:T(8,128)(2,1)S(1)}, u32[]{:S(2)}, u32[]{:S(2)}) async-start(bf16[8,7,1024]{2,1,0:T(8,128)(2,1)} %copy.46), calls=%async_computation.3 | async-start | bytes 262144 | tf_op jit(solution)/shard_map/all_to_all | solution.py:138
  232.0 2.7 %convolution_convert_fusion.2 = bf16[11,2048]{1,0:T(8,128)(2,1)} fusion(bf16[256,2048]{0,1:T(8,128)(2,1)S(1)} %bitcast.77, bf16[11,2048]{1,0:T(8,128)(2,1)S(1)} %fusion.32, bf16[2048,256]{1,0:T(8,128)(2,1)} %all-gather.13.cloned.1.call-done, f32[11,256]{1,0:T(8,128)S(1)} %fusion.67), kind=kOutput, calls=%fused_computation.7 | convolution fusion | flops 23108096 | bytes 2198528 | tf_op jit(solution)/shard_map/dot_general | solution.py:97
  234.7 3.9 %all-to-all-done.1 = bf16[8,7,1024]{2,1,0:T(8,128)(2,1)S(1)} async-done(((bf16[8,7,1024]{2,1,0:T(8,128)(2,1)}), bf16[8,7,1024]{2,1,0:T(8,128)(2,1)S(1)}, u32[]{:S(2)}, u32[]{:S(2)}) %all-to-all-start.1) | async-done | bytes 114720 | tf_op jit(solution)/shard_map/all_to_all | solution.py:138
  239.0 6.3 %reduce-scatter.3.cloned.1.call-done = bf16[11,1024]{1,0:T(8,128)(2,1)} async-done(((bf16[11,2048]{1,0:T(8,128)(2,1)}), bf16[11,1024]{1,0:T(8,128)(2,1)}) %reduce-scatter.3.cloned.1.call-update) | async-done | bytes 22544 | tf_op jit(solution)/shard_map/reduce_scatter | solution.py:102
  245.3 1.4 add_convert_fusion
  (65 shorter events, 3.3 us)
Async XLA Ops:
  7.2 182.2 %copy-start = (bf16[1,256,2048]{2,1,0:T(8,128)(2,1)S(1)}, bf16[1,256,2048]{2,1,0:T(8,128)(2,1)}, u32[]{:S(2)}) copy-start(bf16[1,256,2048]{2,1,0:T(8,128)(2,1)} %param.32) | copy-start | bytes 3145732
  7.2 34.3 %all-gather.7.cloned.1.call-start = ((), (), s32[]{:S(2)}) async-start(), calls=%async_computation.4 | async-start | bytes 2359296 | tf_op jit(solution)/shard_map/all_gather | solution.py:64
  7.9 155.4 %all-gather.9.cloned.1.call-start = ((), (), s32[]{:S(2)}) async-start(), calls=%async_computation.5 | async-start | bytes 2359296 | tf_op jit(solution)/shard_map/all_gather | solution.py:83
  8.7 215.2 %all-gather.15.cloned.1.call-start = ((), (), s32[]{:S(2)}) async-start(), calls=%async_computation.10 | async-start | bytes 1179648 | tf_op jit(solution)/shard_map/all_gather | solution.py:99
  9.4 216.0 %all-gather.11.cloned.1.call-start = ((), (), s32[]{:S(2)}) async-start(), calls=%async_computation.6 | async-start | bytes 1179648 | tf_op jit(solution)/shard_map/all_gather | solution.py:90
  10.0 216.9 %reduce-scatter.5.cloned.1.call-start = ((), (), s32[]{:S(2)}) async-start(), calls=%async_computation.9 | async-start | bytes 344064 | tf_op jit(solution)/shard_map/reduce_scatter | solution.py:133
  11.0 13.0 %copy-start.9 = (s32[11]{0:T(128)S(1)}, s32[11]{0:T(128)}, u32[]{:S(2)}) copy-start(s32[11]{0:T(128)} %param.26) | copy-start | bytes 136
  11.0 13.1 %copy-start.10 = (f32[8]{0:T(128)S(1)}, f32[8]{0:T(128)}, u32[]{:S(2)}) copy-start(f32[8]{0:T(128)} %param.24) | copy-start | bytes 100
  11.0 13.2 %copy-start.7 = (s32[11,4]{0,1:T(4,128)S(1)}, s32[11,4]{0,1:T(4,128)}, u32[]{:S(2)}) copy-start(s32[11,4]{0,1:T(4,128)} %param.28) | copy-start | bytes 532
  11.0 30.5 %copy-start.1 = (bf16[11,2048]{1,0:T(8,128)(2,1)S(1)}, bf16[11,2048]{1,0:T(8,128)(2,1)}, u32[]{:S(2)}) copy-start(bf16[11,2048]{1,0:T(8,128)(2,1)} %param.18) | copy-start | bytes 135172
  11.0 30.5 %copy-start.3 = (f32[2048]{0:T(1024)S(1)}, f32[2048]{0:T(1024)}, u32[]{:S(2)}) copy-start(f32[2048]{0:T(1024)} %param.19) | copy-start | bytes 24580
  158.7 15.6 %copy-start.6 = (f32[2048]{0:T(1024)S(1)}, f32[2048]{0:T(1024)}, u32[]{:S(2)}) copy-start(f32[2048]{0:T(1024)} %param.20) | copy-start | bytes 24580
  158.7 28.7 %copy-start.2 = (bf16[1,2048,256]{2,1,0:T(8,128)(2,1)S(1)}, bf16[1,2048,256]{2,1,0:T(8,128)(2,1)}, u32[]{:S(2)}) copy-start(bf16[1,2048,256]{2,1,0:T(8,128)(2,1)} %param.31) | copy-start | bytes 3145732
  163.2 27.8 %copy-start.8 = (f32[11,4]{0,1:T(4,128)S(1)}, f32[11,4]{0,1:T(4,128)}, u32[]{:S(2)}) copy-start(f32[11,4]{0,1:T(4,128)} %param.29) | copy-start | bytes 532
  163.2 27.9 %copy-start.4 = (bf16[256,128]{1,0:T(8,128)(2,1)S(1)}, bf16[256,128]{1,0:T(8,128)(2,1)}, u32[]{:S(2)}) copy-start(bf16[256,128]{1,0:T(8,128)(2,1)} %param.22) | copy-start | bytes 196612
  163.2 43.1 %copy-start.5 = (bf16[256,128]{1,0:T(8,128)(2,1)S(1)}, bf16[256,128]{1,0:T(8,128)(2,1)}, u32[]{:S(2)}) copy-start(bf16[256,128]{1,0:T(8,128)(2,1)} %param.23) | copy-start | bytes 196612
  190.4 41.6 %all-gather.13.cloned.1.call-start = ((), (), s32[]{:S(2)}) async-start(), calls=%async_computation.7 | async-start | bytes 1179648 | tf_op jit(solution)/shard_map/all_gather | solution.py:91
  228.5 10.1 %all-to-all-start.1 = ((bf16[8,7,1024]{2,1,0:T(8,128)(2,1)}), bf16[8,7,1024]{2,1,0:T(8,128)(2,1)S(1)}, u32[]{:S(2)}, u32[]{:S(2)}) async-start(bf16[8,7,1024]{2,1,0:T(8,128)(2,1)} %copy.46), calls=%async_computation.3 | async-start | bytes 262144 | tf_op jit(solution)/shard_map/all_to_all | solution.py:138
  231.9 13.5 %reduce-scatter.3.cloned.1.call-start = ((), (), s32[]{:S(2)}) async-start(), calls=%async_computation.8 | async-start | bytes 98304 | tf_op jit(solution)/shard_map/reduce_scatter | solution.py:102
Sparse Core Ops, SparseCore 0:
  9.6 31.8 all-gather.6
  43.1 29.9 all-gather.8
  74.7 21.2 all-gather.14
  97.5 22.0 all-gather.10
  190.5 9.3 reduce-scatter.4
  201.3 24.5 all-gather.12
  234.9 10.4 reduce-scatter.2
